TPU v7x, 32 devices: a whole 2x2x4 slice. The times are simulated.
32 devices in a mesh: ep: 8 (over z, x), tp: 4 (over y, core).
Axes of the slice: x: 2, y: 2, z: 4, core: 2. Of those that a mesh axis runs over, the one named last changes fastest.
Arguments:
- conv_gate: bfloat16 [4096, 2048], P('ep', 'tp'), may hold values from -6 to 6
- conv_in_gate: bfloat16 [4096, 2048], P('ep', 'tp'), may hold values from -6 to 6
- conv_value: bfloat16 [4096, 2048], P('ep', 'tp'), may hold values from -6 to 6
- conv_taps: float32 [3, 2048], P(None, 'tp'), may hold values from -3.5 to 3.5
- mix_out_weight: bfloat16 [2048, 4096], P(None, 'tp'), may hold values from -0.125 to 0.125
- expert_input: bfloat16 [1280, 4096], P('ep', 'tp'), may hold values from -1600 to 1600
- expert_gain: float32 [4096], replicated, may hold values from 0.1 to 1.9
- routes: int32 [1280, 2], P('ep'), may hold values from 0 to 7, all different within a row; in each aligned block of 160 rows (0 to 159, 160 to 319, ...) at most 60 rows name the same one
- group_prob: float32 [1280], P('ep'), may hold values from 0.3 to 1
- pair_logits: float32 [1280, 2], P('ep'), may hold values from -6 to 6
- expert_gate: bfloat16 [8, 4096, 2048], P('ep', None, 'tp'), may hold values from -0.09375 to 0.09375
- expert_up: bfloat16 [8, 4096, 2048], P('ep', None, 'tp'), may hold values from -0.09375 to 0.09375
- expert_down: bfloat16 [8, 2048, 4096], P('ep', None, 'tp'), may hold values from -0.125 to 0.125
Outputs:
- mixed: bfloat16 [4096, 4096], P('ep', 'tp')
- expert_output: bfloat16 [1280, 4096], P('ep', 'tp')
Inputs may be any that keep to these rules, and one draw needn't show every extreme that they name: `routes`: in the 160 rows of one index of ep no expert is named by more than 60 rows, a bound that some block reaches; each row names 2 different experts.
All inputs are finite; a program needn't handle non-finite values.
Results may differ from a plain program's by a relative error of at most 0.0071.
Values may be sent and summed in bfloat16 or wider, within the bound.
No kernel may reach another device: no remote copies, remote signals or barrier semaphores. Data moves between devices by JAX's collectives and lax.ppermute only.
A program may use at most 64 MiB of HBM per device.

v0:
```python
import jax
import jax.numpy as jnp
from jax import lax
from jax.sharding import PartitionSpec as P

D = 4096
EPS = 1e-06


def shifted(block, axis, distance):
    devices = range(lax.axis_size(axis))
    route = [(i - distance, i) for i in devices if i - distance in devices]
    return lax.ppermute(block, axis, route)


def slot_table(route_block, capacity, expert_count):
    pair_ids = route_block.reshape(-1)
    onehot = (pair_ids[:, None] == jnp.arange(expert_count, dtype=jnp.int32)[None, :]).astype(
        jnp.int32
    )
    earlier = jnp.cumsum(onehot, axis=0) - onehot
    within = jnp.sum(earlier * onehot, axis=1)
    return pair_ids * capacity + within


def pair_weights(group_prob, pair_logits):
    spread = pair_logits[:, 0] - pair_logits[:, 1]
    return (
        jnp.stack([jax.nn.sigmoid(spread), jax.nn.sigmoid(-spread)], axis=1) * group_prob[:, None]
    )


def per_device(
    conv_gate,
    conv_in_gate,
    conv_value,
    conv_taps,
    mix_out_weight,
    expert_input,
    expert_gain,
    routes,
    group_prob,
    pair_logits,
    expert_gate,
    expert_up,
    expert_down,
):
    reach = conv_taps.shape[0] - 1
    token_rows = conv_value.shape[0]
    products = conv_in_gate.astype(jnp.float32) * conv_value.astype(jnp.float32)
    earlier_rows = shifted(products[token_rows - reach :], "ep", 1)
    padded = jnp.concatenate([earlier_rows, products], axis=0)
    convolved = jnp.zeros_like(products)
    for offset in range(reach + 1):
        convolved = convolved + conv_taps[offset][None, :] * padded[offset : offset + token_rows]
    mixer_rows = (conv_gate.astype(jnp.float32) * convolved).astype(jnp.bfloat16)
    mixed = jnp.dot(
        lax.all_gather(mixer_rows, "tp", axis=1, tiled=True),
        mix_out_weight,
        preferred_element_type=jnp.float32,
    ).astype(jnp.bfloat16)
    expert_count = lax.axis_size("ep")
    tok_rows, choose_count = routes.shape
    capacity = 3 * tok_rows * choose_count // (2 * expert_count)
    slot_index = slot_table(routes, capacity, expert_count)
    pair_row = jnp.arange(tok_rows * choose_count, dtype=jnp.int32) // choose_count
    slot_rows = expert_count * capacity
    gate_block = expert_gate[0]
    up_block = expert_up[0]
    down_block = expert_down[0]
    columns = expert_input.shape[1]
    features = expert_input.astype(jnp.float32)
    squares = lax.psum(jnp.sum(features * features, axis=1), "tp")
    scale = lax.rsqrt(squares / D + EPS)
    gain_part = lax.dynamic_slice_in_dim(expert_gain, lax.axis_index("tp") * columns, columns, 0)
    normed = (features * scale[:, None] * gain_part[None, :]).astype(jnp.bfloat16)
    buffer = jnp.zeros((slot_rows, columns), jnp.bfloat16).at[slot_index].set(normed[pair_row])
    arrived = lax.all_to_all(
        buffer.reshape(expert_count, capacity, columns),
        "ep",
        split_axis=0,
        concat_axis=0,
        tiled=True,
    ).reshape(slot_rows, columns)
    shard_piece = lax.all_gather(arrived, "tp", axis=1, tiled=True)
    gate_sum = jnp.dot(shard_piece, gate_block, preferred_element_type=jnp.float32)
    up_sum = jnp.dot(shard_piece, up_block, preferred_element_type=jnp.float32)
    hidden = (jax.nn.silu(gate_sum) * up_sum).astype(jnp.bfloat16)
    results = jnp.dot(
        lax.all_gather(hidden, "tp", axis=1, tiled=True),
        down_block,
        preferred_element_type=jnp.float32,
    ).astype(jnp.bfloat16)
    returned = lax.all_to_all(
        results.reshape(expert_count, capacity, down_block.shape[1]),
        "ep",
        split_axis=0,
        concat_axis=0,
        tiled=True,
    ).reshape(slot_rows, down_block.shape[1])
    picked = (
        returned[slot_index]
        .reshape(tok_rows, choose_count, down_block.shape[1])
        .astype(jnp.float32)
    )
    weights = pair_weights(group_prob, pair_logits)
    expert_output = jnp.sum(picked * weights[:, :, None], axis=1).astype(jnp.bfloat16)
    return (mixed, expert_output)


def solution(mesh):
    in_specs = (
        P("ep", "tp"),
        P("ep", "tp"),
        P("ep", "tp"),
        P(None, "tp"),
        P(None, "tp"),
        P("ep", "tp"),
        P(),
        P("ep", None),
        P("ep"),
        P("ep", None),
        P("ep", None, "tp"),
        P("ep", None, "tp"),
        P("ep", None, "tp"),
    )
    out_specs = (P("ep", "tp"), P("ep", "tp"))
    return jax.shard_map(
        per_device, mesh=mesh, in_specs=in_specs, out_specs=out_specs, check_vma=False
    )
```

profile of v0, /device:TPU:0, one launch (start us, length us, event | category | flops | bytes accessed | tf_op | source)
XLA Modules:
  0.0 170.7 jit_solution(3366997663291530493)
XLA Ops:
  7.2 0.8 copy.17
  8.9 0.9 reduce-window.6
  10.4 1.1 fusion.22
  11.5 8.4 %psum.7 = f32[160]{0:T(256)S(1)} all-reduce(f32[160]{0:T(256)S(1)} %fusion.22), channel_id=1, replica_groups=mesh['ep'=8,'tp'=4] {'tp'}, use_global_device_ids=true, to_apply=%region_4.5 | all-reduce | flops 160 | bytes 1280 | tf_op jit(solution)/shard_map/psum | solution.py:73
  20.6 1.1 fusion.24
  21.8 4.5 %scatter_custom_fusion = bf16[480,1024]{1,0:T(8,128)(2,1)S(1)} fusion(s32[320]{0:T(512)S(1)} %fusion.30, bf16[160,1024]{1,0:T(8,128)(2,1)S(1)} %fusion.24, s32[1024]{0:T(1024)S(1)} %pad_clamp_fusion.1, bf16[]{:T(256)} %constant.18.clone.1), kind=kCustom, calls=%fused_computation.30 | custom fusion | bytes 983042 | tf_op jit(solution)/shard_map/scatter | solution.py:77
  26.4 30.1 %all_to_all.10 = bf16[8,60,1024]{2,1,0:T(8,128)(2,1)S(1)} all-to-all(bf16[8,60,1024]{2,1,0:T(8,128)(2,1)S(1)} %reshape.137), channel_id=1, replica_groups=mesh['ep'=8,'tp'=4] {'ep'}, dimensions={0} | all-to-all | bytes 1966080 | tf_op jit(solution)/shard_map/all_to_all | solution.py:78
  56.6 1.1 reshape.138
  57.8 32.1 %all-gather.6.cloned.1.call-done = bf16[480,4096]{1,0:T(8,128)(2,1)} async-done(((bf16[480,1024]{1,0:T(8,128)(2,1)}), bf16[480,4096]{1,0:T(8,128)(2,1)}) %all-gather.6.cloned.1.call-update) | async-done | bytes 3932176 | tf_op jit(solution)/shard_map/all_gather | solution.py:85
  89.9 5.7 %fusion.4 = f32[480,512]{1,0:T(8,128)S(1)} fusion(bf16[480,4096]{1,0:T(8,128)(2,1)} %all-gather.6.cloned.1.call-done, bf16[1,4096,512]{2,1,0:T(8,128)(2,1)} %param.23), kind=kOutput, calls=%fused_computation.7 | convolution fusion | flops 2013265920 | bytes 9109504 | tf_op jit(solution)/shard_map/dot_general | solution.py:86
  95.7 3.0 %fusion.12 = bf16[480,512]{1,0:T(8,128)(2,1)} fusion(bf16[480,4096]{1,0:T(8,128)(2,1)S(1)} %copy-done.7, bf16[1,4096,512]{2,1,0:T(8,128)(2,1)S(1)} %copy-done.6, f32[480,512]{1,0:T(8,128)S(1)} %fusion.4), kind=kOutput, calls=%fused_computation.13 | convolution fusion | flops 2014740480 | bytes 9601024 | tf_op jit(solution)/shard_map/dot_general | solution.py:87
  99.0 3.4 %collective-permute-start = (f32[2,512]{1,0:T(2,128)S(1)}, f32[2,512]{1,0:T(2,128)S(1)}, u32[]{:S(2)}, u32[]{:S(2)}) collective-permute-start(f32[2,512]{1,0:T(2,128)S(1)} %slice.48), channel_id=1, source_target_pairs={{0,4},{4,8},{8,12},{12,16},{16,20},{20,24},{24,28},{1,5},{5,9},{9,... | collective-permute-start | bytes 12296 | tf_op jit(solution)/shard_map/ppermute | solution.py:13
  102.4 1.3 collective-permute-done
  103.7 1.2 fusion.20
  104.9 15.8 %all-gather.8.cloned.1.call-done = bf16[480,2048]{1,0:T(8,128)(2,1)} async-done(((bf16[480,512]{1,0:T(8,128)(2,1)}), bf16[480,2048]{1,0:T(8,128)(2,1)}) %all-gather.8.cloned.1.call-update) | async-done | bytes 1966096 | tf_op jit(solution)/shard_map/all_gather | solution.py:90
  120.8 5.0 %fusion.6 = bf16[480,1024]{1,0:T(8,128)(2,1)S(1)} fusion(bf16[480,2048]{1,0:T(8,128)(2,1)} %all-gather.8.cloned.1.call-done, bf16[1,2048,1024]{2,1,0:T(8,128)(2,1)} %param.25), kind=kOutput, calls=%fused_computation.10 | convolution fusion | flops 2013757440 | bytes 7143424 | tf_op jit(solution)/shard_map/dot_general | solution.py:89
  125.8 1.2 reshape.139
  126.9 5.5 %all-to-all-start.1 = ((bf16[8,60,1024]{2,1,0:T(8,128)(2,1)}), bf16[8,60,1024]{2,1,0:T(8,128)(2,1)S(1)}, u32[]{:S(2)}, u32[]{:S(2)}) async-start(bf16[8,60,1024]{2,1,0:T(8,128)(2,1)} %reshape.139), calls=%async_computation.1 | async-start | bytes 2097152 | tf_op jit(solution)/shard_map/all_to_all | solution.py:94
  132.6 12.9 %all-gather.4.cloned.1.call-done = bf16[512,2048]{1,0:T(8,128)(2,1)} async-done(((bf16[512,512]{1,0:T(8,128)(2,1)}), bf16[512,2048]{1,0:T(8,128)(2,1)}) %all-gather.4.cloned.1.call-update) | async-done | bytes 2097168 | tf_op jit(solution)/shard_map/all_gather | solution.py:58
  145.5 6.1 %convolution_convert_fusion = bf16[512,1024]{1,0:T(8,128)(2,1)} fusion(bf16[512,2048]{1,0:T(8,128)(2,1)} %all-gather.4.cloned.1.call-done, bf16[2048,1024]{1,0:T(8,128)(2,1)} %param.17), kind=kOutput, calls=%fused_computation.9 | convolution fusion | flops 2148007936 | bytes 7340032 | tf_op jit(solution)/shard_map/dot_general | solution.py:57
  151.6 7.0 %all-to-all-done.1 = bf16[8,60,1024]{2,1,0:T(8,128)(2,1)S(1)} async-done(((bf16[8,60,1024]{2,1,0:T(8,128)(2,1)}), bf16[8,60,1024]{2,1,0:T(8,128)(2,1)S(1)}, u32[]{:S(2)}, u32[]{:S(2)}) %all-to-all-start.1) | async-done | bytes 983072 | tf_op jit(solution)/shard_map/all_to_all | solution.py:94
  158.8 2.1 %gather_fusion = bf16[320,1024]{1,0:T(8,128)(2,1)S(1)} fusion(bf16[480,1024]{1,0:T(8,128)(2,1)S(1)} %reshape.140, s32[1024]{0:T(1024)S(1)} %pad_clamp_fusion), kind=kCustom, calls=%fused_computation.1 | custom fusion | bytes 1312000 | tf_op jit(solution)/shard_map/gather | solution.py:102
  160.9 0.8 reshape.142
  161.7 2.4 %multiply_reduce_fusion = bf16[160,1024]{1,0:T(8,128)(2,1)} fusion(f32[160,2,1024]{2,1,0:T(2,128)S(1)} %reshape.142, f32[160,2]{1,0:T(8,128)S(1)} %copy.18), kind=kLoop, calls=%fused_computation.12 | loop fusion | flops 491520 | bytes 1639680 | tf_op jit(solution)/shard_map/reduce_sum | solution.py:107
  (47 shorter events, 3.1 us)
Async XLA Ops:
  7.2 82.8 %all-gather.6.cloned.1.call-start = ((), (), s32[]{:S(2)}) async-start(), calls=%async_computation.3 | async-start | bytes 4915200 | tf_op jit(solution)/shard_map/all_gather | solution.py:85
  57.7 63.0 %all-gather.8.cloned.1.call-start = ((), (), s32[]{:S(2)}) async-start(), calls=%async_computation.4 | async-start | bytes 2457600 | tf_op jit(solution)/shard_map/all_gather | solution.py:90
  89.9 5.7 %copy-start.6 = (bf16[1,4096,512]{2,1,0:T(8,128)(2,1)S(1)}, bf16[1,4096,512]{2,1,0:T(8,128)(2,1)}, u32[]{:S(2)}) copy-start(bf16[1,4096,512]{2,1,0:T(8,128)(2,1)} %param.24) | copy-start | bytes 12582916
  89.9 5.8 %copy-start.7 = (bf16[480,4096]{1,0:T(8,128)(2,1)S(1)}, bf16[480,4096]{1,0:T(8,128)(2,1)}, u32[]{:S(2)}) copy-start(bf16[480,4096]{1,0:T(8,128)(2,1)} %all-gather.6.cloned.1.call-done) | copy-start | bytes 11796484
  95.7 3.1 %copy-start.1 = (bf16[512,512]{1,0:T(8,128)(2,1)S(1)}, bf16[512,512]{1,0:T(8,128)(2,1)}, u32[]{:S(2)}) copy-start(bf16[512,512]{1,0:T(8,128)(2,1)} %param.15) | copy-start | bytes 1572868
  95.7 3.1 %copy-start.2 = (bf16[512,512]{1,0:T(8,128)(2,1)S(1)}, bf16[512,512]{1,0:T(8,128)(2,1)}, u32[]{:S(2)}) copy-start(bf16[512,512]{1,0:T(8,128)(2,1)} %param.14) | copy-start | bytes 1572868
  95.7 6.7 %copy-start.3 = (f32[3,512]{1,0:T(4,128)S(1)}, f32[3,512]{1,0:T(4,128)}, u32[]{:S(2)}) copy-start(f32[3,512]{1,0:T(4,128)} %param.16) | copy-start | bytes 18436
  95.7 8.0 %copy-start = (bf16[512,512]{1,0:T(8,128)(2,1)S(1)}, bf16[512,512]{1,0:T(8,128)(2,1)}, u32[]{:S(2)}) copy-start(bf16[512,512]{1,0:T(8,128)(2,1)} %param.13) | copy-start | bytes 1572868
  98.8 46.7 %all-gather.4.cloned.1.call-start = ((), (), s32[]{:S(2)}) async-start(), calls=%async_computation.2 | async-start | bytes 2621440 | tf_op jit(solution)/shard_map/all_gather | solution.py:58
  99.0 4.7 %collective-permute-start = (f32[2,512]{1,0:T(2,128)S(1)}, f32[2,512]{1,0:T(2,128)S(1)}, u32[]{:S(2)}, u32[]{:S(2)}) collective-permute-start(f32[2,512]{1,0:T(2,128)S(1)} %slice.48), channel_id=1, source_target_pairs={{0,4},{4,8},{8,12},{12,16},{16,20},{20,24},{24,28},{1,5},{5,9},{9,... | collective-permute-start | bytes 12296 | tf_op jit(solution)/shard_map/ppermute | solution.py:13
  125.7 6.7 %copy-start.4 = (f32[160,2]{0,1:T(2,128)S(1)}, f32[160,2]{0,1:T(2,128)}, u32[]{:S(2)}) copy-start(f32[160,2]{0,1:T(2,128)} %param.22) | copy-start | bytes 3844
  125.8 6.7 %copy-start.5 = (f32[160]{0:T(256)S(1)}, f32[160]{0:T(256)}, u32[]{:S(2)}) copy-start(f32[160]{0:T(256)} %param.21) | copy-start | bytes 1924
  126.9 31.7 %all-to-all-start.1 = ((bf16[8,60,1024]{2,1,0:T(8,128)(2,1)}), bf16[8,60,1024]{2,1,0:T(8,128)(2,1)S(1)}, u32[]{:S(2)}, u32[]{:S(2)}) async-start(bf16[8,60,1024]{2,1,0:T(8,128)(2,1)} %reshape.139), calls=%async_computation.1 | async-start | bytes 2097152 | tf_op jit(solution)/shard_map/all_to_all | solution.py:94
Sparse Core Ops, SparseCore 0:
  57.8 32.0 all-gather.5
  98.9 21.8 all-gather.7
  122.9 22.5 all-gather.3
where the time goes:
time: 171 us
  waiting for transfers between devices  69.2 us (40%)
  blocking collectives  38.5 us (23%)
  matrix products  19.9 us (12%)
  between operations  14 us (8%)
  local copies, waits for them, and re-layouts  12.3 us (7%)
  starting transfers between devices  9 us (5%)
  other arithmetic  7.81 us (5%)
    all_gather x1, waiting for transfers between devices, per_device(): shard_piece = lax.all_gather(arrived, 'tp', axis=1, tiled=True)  32.1 us
    all_to_all x1, blocking collectives, per_device(): lax.all_to_all(buffer.reshape(expert_count, capacity, columns), 'ep', spl...  30.1 us
    all_gather x1, waiting for transfers between devices, per_device(): lax.all_gather(hidden, 'tp', axis=1, tiled=True)  15.8 us
    all_gather x1, waiting for transfers between devices, per_device(): lax.all_gather(mixer_rows, 'tp', axis=1, tiled=True)  12.9 us
    psum x1, blocking collectives, per_device(): squares = lax.psum(jnp.sum(features * features, axis=1), 'tp')  8.39 us
    all_to_all x1, waiting for transfers between devices, per_device(): lax.all_to_all(results.reshape(expert_count, capacity, down_block.shape[1...  6.98 us
    dot_general x1, matrix products, per_device(): jnp.dot(lax.all_gather(mixer_rows, 'tp', axis=1, tiled=True), mix_out_wei...  6.12 us
    dot_general x1, matrix products, per_device(): jnp.dot(shard_piece, gate_block, preferred_element_type=jnp.float32)  5.71 us
  transfers between devices with their start and end apart: 5, of which 5 were waited for; matrix products, arithmetic and copies ran while one was open for 8% of the time, Pallas kernels for 0%

commit v1 on v0

--- a/solution.py
+++ b/solution.py
@@ -82,7 +82,8 @@
         concat_axis=0,
         tiled=True,
     ).reshape(slot_rows, columns)
-    shard_piece = lax.all_gather(arrived, "tp", axis=1, tiled=True)
+    blocks = lax.all_gather(arrived, "tp", axis=0, tiled=False)
+    shard_piece = jnp.concatenate(blocks, axis=1)
     gate_sum = jnp.dot(shard_piece, gate_block, preferred_element_type=jnp.float32)
     up_sum = jnp.dot(shard_piece, up_block, preferred_element_type=jnp.float32)
     hidden = (jax.nn.silu(gate_sum) * up_sum).astype(jnp.bfloat16)

time: 171 us -> 171 us (level)
  matrix products: 19.9 us -> 16.3 us
  local copies, waits for them, and re-layouts: 12.3 us -> 15.6 us
    dot_general x1, matrix products: 5.71 us -> 2.19 us  [per_device(): jnp.dot(shard_piece, gate_block, preferred_element_type=jnp.float32)]
where the time goes in v1:
time: 171 us; the launch traced here: 170 us
  waiting for transfers between devices  69.2 us (40%)
  blocking collectives  38.5 us (23%)
  matrix products  16.3 us (10%)
  local copies, waits for them, and re-layouts  15.6 us (9%)
  between operations  14 us (8%)
  starting transfers between devices  9 us (5%)
  other arithmetic  7.81 us (5%)
    all_gather x1, waiting for transfers between devices, per_device(): blocks = lax.all_gather(arrived, 'tp', axis=0, tiled=False)  32.1 us
    all_to_all x1, blocking collectives, per_device(): lax.all_to_all(buffer.reshape(expert_count, capacity, columns), 'ep', spl...  30.1 us
    all_gather x1, waiting for transfers between devices, per_device(): lax.all_gather(hidden, 'tp', axis=1, tiled=True)  15.8 us
    all_gather x1, waiting for transfers between devices, per_device(): lax.all_gather(mixer_rows, 'tp', axis=1, tiled=True)  12.9 us
    psum x1, blocking collectives, per_device(): squares = lax.psum(jnp.sum(features * features, axis=1), 'tp')  8.39 us
    all_to_all x1, waiting for transfers between devices, per_device(): lax.all_to_all(results.reshape(expert_count, capacity, down_block.shape[1...  6.98 us
    dot_general x1, matrix products, per_device(): jnp.dot(lax.all_gather(mixer_rows, 'tp', axis=1, tiled=True), mix_out_wei...  6.12 us
    all_to_all x1, starting transfers between devices, per_device(): lax.all_to_all(results.reshape(expert_count, capacity, down_block.shape[1...  5.51 us
  transfers between devices with their start and end apart: 5, of which 5 were waited for; matrix products, arithmetic and copies ran while one was open for 8% of the time, Pallas kernels for 0%

profile of v1, /device:TPU:0, one launch (start us, length us, event | category | flops | bytes accessed | tf_op | source)
XLA Modules:
  0.0 170.5 jit_solution(1417168286894958634)
XLA Ops:
  8.9 0.9 reduce-window.6
  10.4 1.1 fusion.22
  11.5 8.4 %psum.7 = f32[160]{0:T(256)S(1)} all-reduce(f32[160]{0:T(256)S(1)} %fusion.22), channel_id=1, replica_groups=mesh['ep'=8,'tp'=4] {'tp'}, use_global_device_ids=true, to_apply=%region_4.5 | all-reduce | flops 160 | bytes 1280 | tf_op jit(solution)/shard_map/psum | solution.py:73
  20.6 1.1 fusion.24
  21.8 4.5 %scatter_custom_fusion = bf16[480,1024]{1,0:T(8,128)(2,1)S(1)} fusion(s32[320]{0:T(512)S(1)} %fusion.30, bf16[160,1024]{1,0:T(8,128)(2,1)S(1)} %fusion.24, s32[1024]{0:T(1024)S(1)} %pad_clamp_fusion.1, bf16[]{:T(256)} %constant.18.clone.1), kind=kCustom, calls=%fused_computation.30 | custom fusion | bytes 983042 | tf_op jit(solution)/shard_map/scatter | solution.py:77
  26.4 30.1 %all_to_all.10 = bf16[8,60,1024]{2,1,0:T(8,128)(2,1)S(1)} all-to-all(bf16[8,60,1024]{2,1,0:T(8,128)(2,1)S(1)} %reshape.140), channel_id=1, replica_groups=mesh['ep'=8,'tp'=4] {'ep'}, dimensions={0} | all-to-all | bytes 1966080 | tf_op jit(solution)/shard_map/all_to_all | solution.py:78
  56.6 1.1 all_gather_reshape.3
  57.8 32.1 %all-gather.6.cloned.1.call-done = bf16[4,480,1024]{2,1,0:T(8,128)(2,1)} async-done(((bf16[1,480,1024]{2,1,0:T(8,128)(2,1)}), bf16[4,480,1024]{2,1,0:T(8,128)(2,1)}) %all-gather.6.cloned.1.call-update) | async-done | bytes 3932176 | tf_op jit(solution)/shard_map/all_gather | solution.py:85
  89.9 2.7 %copy.24 = bf16[4,60,8,1024]{3,2,0,1:T(8,128)(2,1)S(1)} copy(bf16[4,60,8,1024]{3,2,1,0:T(8,128)(2,1)} %bitcast.33) | data formatting | bytes 7864320 | tf_op jit(solution)/shard_map/reshape | solution.py:86
  93.3 2.2 %fusion.4 = f32[480,512]{1,0:T(8,128)S(1)} fusion(bf16[480,4096]{1,0:T(8,128)(2,1)S(1)} %bitcast.34, bf16[1,4096,512]{2,1,0:T(8,128)(2,1)S(1)} %copy-done.6), kind=kOutput, calls=%fused_computation.7 | convolution fusion | flops 2013265920 | bytes 9109504 | tf_op jit(solution)/shard_map/dot_general | solution.py:87
  95.5 3.0 %fusion.12 = bf16[480,512]{1,0:T(8,128)(2,1)} fusion(bf16[480,4096]{1,0:T(8,128)(2,1)S(1)} %bitcast.35, bf16[1,4096,512]{2,1,0:T(8,128)(2,1)S(1)} %copy-done.7, f32[480,512]{1,0:T(8,128)S(1)} %fusion.4), kind=kOutput, calls=%fused_computation.13 | convolution fusion | flops 2014740480 | bytes 9601024 | tf_op jit(solution)/shard_map/dot_general | solution.py:88
  98.8 3.4 %collective-permute-start = (f32[2,512]{1,0:T(2,128)S(1)}, f32[2,512]{1,0:T(2,128)S(1)}, u32[]{:S(2)}, u32[]{:S(2)}) collective-permute-start(f32[2,512]{1,0:T(2,128)S(1)} %slice.48), channel_id=1, source_target_pairs={{0,4},{4,8},{8,12},{12,16},{16,20},{20,24},{24,28},{1,5},{5,9},{9,... | collective-permute-start | bytes 12296 | tf_op jit(solution)/shard_map/ppermute | solution.py:13
  102.3 1.3 collective-permute-done
  103.5 1.2 fusion.20
  104.8 15.8 %all-gather.8.cloned.1.call-done = bf16[480,2048]{1,0:T(8,128)(2,1)} async-done(((bf16[480,512]{1,0:T(8,128)(2,1)}), bf16[480,2048]{1,0:T(8,128)(2,1)}) %all-gather.8.cloned.1.call-update) | async-done | bytes 1966096 | tf_op jit(solution)/shard_map/all_gather | solution.py:91
  120.6 5.0 %fusion.6 = bf16[480,1024]{1,0:T(8,128)(2,1)S(1)} fusion(bf16[480,2048]{1,0:T(8,128)(2,1)} %all-gather.8.cloned.1.call-done, bf16[1,2048,1024]{2,1,0:T(8,128)(2,1)} %param.25), kind=kOutput, calls=%fused_computation.10 | convolution fusion | flops 2013757440 | bytes 7143424 | tf_op jit(solution)/shard_map/dot_general | solution.py:90
  125.6 1.2 reshape.143
  126.8 5.5 %all-to-all-start.1 = ((bf16[8,60,1024]{2,1,0:T(8,128)(2,1)}), bf16[8,60,1024]{2,1,0:T(8,128)(2,1)S(1)}, u32[]{:S(2)}, u32[]{:S(2)}) async-start(bf16[8,60,1024]{2,1,0:T(8,128)(2,1)} %reshape.143), calls=%async_computation.1 | async-start | bytes 2097152 | tf_op jit(solution)/shard_map/all_to_all | solution.py:95
  132.5 12.9 %all-gather.4.cloned.1.call-done = bf16[512,2048]{1,0:T(8,128)(2,1)} async-done(((bf16[512,512]{1,0:T(8,128)(2,1)}), bf16[512,2048]{1,0:T(8,128)(2,1)}) %all-gather.4.cloned.1.call-update) | async-done | bytes 2097168 | tf_op jit(solution)/shard_map/all_gather | solution.py:58
  145.3 6.1 %convolution_convert_fusion = bf16[512,1024]{1,0:T(8,128)(2,1)} fusion(bf16[512,2048]{1,0:T(8,128)(2,1)} %all-gather.4.cloned.1.call-done, bf16[2048,1024]{1,0:T(8,128)(2,1)} %param.17), kind=kOutput, calls=%fused_computation.9 | convolution fusion | flops 2148007936 | bytes 7340032 | tf_op jit(solution)/shard_map/dot_general | solution.py:57
  151.5 7.0 %all-to-all-done.1 = bf16[8,60,1024]{2,1,0:T(8,128)(2,1)S(1)} async-done(((bf16[8,60,1024]{2,1,0:T(8,128)(2,1)}), bf16[8,60,1024]{2,1,0:T(8,128)(2,1)S(1)}, u32[]{:S(2)}, u32[]{:S(2)}) %all-to-all-start.1) | async-done | bytes 983072 | tf_op jit(solution)/shard_map/all_to_all | solution.py:95
  158.6 2.1 %gather_fusion = bf16[320,1024]{1,0:T(8,128)(2,1)S(1)} fusion(bf16[480,1024]{1,0:T(8,128)(2,1)S(1)} %reshape.144, s32[1024]{0:T(1024)S(1)} %pad_clamp_fusion), kind=kCustom, calls=%fused_computation.1 | custom fusion | bytes 1312000 | tf_op jit(solution)/shard_map/gather | solution.py:103
  160.7 0.8 reshape.146
  161.5 2.4 %multiply_reduce_fusion = bf16[160,1024]{1,0:T(8,128)(2,1)} fusion(f32[160,2,1024]{2,1,0:T(2,128)S(1)} %reshape.146, f32[160,2]{1,0:T(8,128)S(1)} %copy.23), kind=kLoop, calls=%fused_computation.12 | loop fusion | flops 491520 | bytes 1639680 | tf_op jit(solution)/shard_map/reduce_sum | solution.py:108
  (48 shorter events, 4.5 us)
Async XLA Ops:
  7.2 82.8 %all-gather.6.cloned.1.call-start = ((), (), s32[]{:S(2)}) async-start(), calls=%async_computation.3 | async-start | bytes 4915200 | tf_op jit(solution)/shard_map/all_gather | solution.py:85
  57.7 62.9 %all-gather.8.cloned.1.call-start = ((), (), s32[]{:S(2)}) async-start(), calls=%async_computation.4 | async-start | bytes 2457600 | tf_op jit(solution)/shard_map/all_gather | solution.py:91
  89.9 3.4 %copy-start.6 = (bf16[1,4096,512]{2,1,0:T(8,128)(2,1)S(1)}, bf16[1,4096,512]{2,1,0:T(8,128)(2,1)}, u32[]{:S(2)}) copy-start(bf16[1,4096,512]{2,1,0:T(8,128)(2,1)} %param.23) | copy-start | bytes 12582916
  93.3 2.2 %copy-start.7 = (bf16[1,4096,512]{2,1,0:T(8,128)(2,1)S(1)}, bf16[1,4096,512]{2,1,0:T(8,128)(2,1)}, u32[]{:S(2)}) copy-start(bf16[1,4096,512]{2,1,0:T(8,128)(2,1)} %param.24) | copy-start | bytes 12582916
  95.5 3.2 %copy-start.1 = (bf16[512,512]{1,0:T(8,128)(2,1)S(1)}, bf16[512,512]{1,0:T(8,128)(2,1)}, u32[]{:S(2)}) copy-start(bf16[512,512]{1,0:T(8,128)(2,1)} %param.15) | copy-start | bytes 1572868
  95.5 3.2 %copy-start.2 = (bf16[512,512]{1,0:T(8,128)(2,1)S(1)}, bf16[512,512]{1,0:T(8,128)(2,1)}, u32[]{:S(2)}) copy-start(bf16[512,512]{1,0:T(8,128)(2,1)} %param.14) | copy-start | bytes 1572868
  95.5 6.7 %copy-start.3 = (f32[3,512]{1,0:T(4,128)S(1)}, f32[3,512]{1,0:T(4,128)}, u32[]{:S(2)}) copy-start(f32[3,512]{1,0:T(4,128)} %param.16) | copy-start | bytes 18436
  95.5 8.0 %copy-start = (bf16[512,512]{1,0:T(8,128)(2,1)S(1)}, bf16[512,512]{1,0:T(8,128)(2,1)}, u32[]{:S(2)}) copy-start(bf16[512,512]{1,0:T(8,128)(2,1)} %param.13) | copy-start | bytes 1572868
  98.6 46.7 %all-gather.4.cloned.1.call-start = ((), (), s32[]{:S(2)}) async-start(), calls=%async_computation.2 | async-start | bytes 2621440 | tf_op jit(solution)/shard_map/all_gather | solution.py:58
  98.8 4.7 %collective-permute-start = (f32[2,512]{1,0:T(2,128)S(1)}, f32[2,512]{1,0:T(2,128)S(1)}, u32[]{:S(2)}, u32[]{:S(2)}) collective-permute-start(f32[2,512]{1,0:T(2,128)S(1)} %slice.48), channel_id=1, source_target_pairs={{0,4},{4,8},{8,12},{12,16},{16,20},{20,24},{24,28},{1,5},{5,9},{9,... | collective-permute-start | bytes 12296 | tf_op jit(solution)/shard_map/ppermute | solution.py:13
  125.6 6.7 %copy-start.4 = (f32[160,2]{0,1:T(2,128)S(1)}, f32[160,2]{0,1:T(2,128)}, u32[]{:S(2)}) copy-start(f32[160,2]{0,1:T(2,128)} %param.22) | copy-start | bytes 3844
  125.6 6.7 %copy-start.5 = (f32[160]{0:T(256)S(1)}, f32[160]{0:T(256)}, u32[]{:S(2)}) copy-start(f32[160]{0:T(256)} %param.21) | copy-start | bytes 1924
  126.8 31.7 %all-to-all-start.1 = ((bf16[8,60,1024]{2,1,0:T(8,128)(2,1)}), bf16[8,60,1024]{2,1,0:T(8,128)(2,1)S(1)}, u32[]{:S(2)}, u32[]{:S(2)}) async-start(bf16[8,60,1024]{2,1,0:T(8,128)(2,1)} %reshape.143), calls=%async_computation.1 | async-start | bytes 2097152 | tf_op jit(solution)/shard_map/all_to_all | solution.py:95
Sparse Core Ops, SparseCore 0:
  57.8 32.0 all-gather.5
  98.7 21.8 all-gather.7
  122.7 22.5 all-gather.3
